TPU v7x, 256 devices: a whole 4x4x8 slice. The times are simulated.
256 devices in a mesh: sp: 32 (over z, y), dp: 8 (over x, core).
Axes of the slice: x: 4, y: 4, z: 8, core: 2. Of those that a mesh axis runs over, the one named last changes fastest.
Arguments:
- queries: bfloat16 [32768, 6144], P(('dp', 'sp')), may hold values from -360 to 360
- latent: bfloat16 [32768, 1024], P(('dp', 'sp')), may hold values from -6 to 6
- rope_key: bfloat16 [32768, 64], P(('dp', 'sp')), may hold values from -6 to 6
- latent_gain: float32 [1024], replicated, may hold values from 0.1 to 1.9
- kv_weight: bfloat16 [1024, 8192], P(None, 'dp'), may hold values from -0.1875 to 0.1875
- gate: bfloat16 [32768, 4096], P(('dp', 'sp')), may hold values from -6 to 6
- out_gain: float32 [4096], replicated, may hold values from 0.1 to 1.9
Outputs:
- attended: bfloat16 [32768, 4096], P(('dp', 'sp'))
All inputs are finite; a program needn't handle non-finite values.
Results may differ from a plain program's by a relative error of at most 0.007.
Values may be sent and summed in bfloat16 or wider, within the bound.
A program may use at most 128 MiB of HBM per device.

v0:
```python
import jax
import jax.numpy as jnp
from jax import lax
from jax.sharding import PartitionSpec as P

HEADS = 32
NOPE = 128
ROPE = 64
VDIM = 128
EPS = 1e-06
THETA = 10000.0


def in_order(blocks, dim):
    blocks = jnp.moveaxis(blocks, 0, dim)
    shape = blocks.shape
    return blocks.reshape(*shape[:dim], shape[dim] * shape[dim + 1], *shape[dim + 2 :])


def copy_for_each(value, axis):
    length = lax.axis_size(axis)
    return lax.all_to_all(
        jnp.broadcast_to(value[None], (length, *value.shape)), axis, 0, 0, tiled=True
    )


def gathered_copies(value, axis, dim):
    return in_order(copy_for_each(value, axis), dim)


def rotary(values, position):
    half_width = values.shape[-1] // 2
    inverse = THETA ** (-jnp.arange(half_width, dtype=jnp.float32) / half_width)
    angles = position.astype(jnp.float32)[:, None] * inverse[None, :]
    if values.ndim == 3:
        angles = angles[:, None, :]
    cosine = jnp.cos(angles)
    sine_part = jnp.sin(angles)
    front_half = values[..., :half_width].astype(jnp.float32)
    back_half = values[..., half_width:].astype(jnp.float32)
    turned = jnp.concatenate(
        [front_half * cosine - back_half * sine_part, back_half * cosine + front_half * sine_part],
        axis=-1,
    )
    return turned.astype(jnp.bfloat16)


def attend(query_block, keys_plain, keys_rotated, values):
    scores = jnp.einsum(
        "qhd,khd->hqk", query_block[..., :NOPE], keys_plain, preferred_element_type=jnp.float32
    )
    scores = scores + jnp.einsum(
        "qhr,kr->hqk", query_block[..., NOPE:], keys_rotated, preferred_element_type=jnp.float32
    )
    scores = scores * (NOPE + ROPE) ** (-0.5)
    row_max = jnp.max(scores, axis=-1, keepdims=True)
    raised = jnp.exp(scores - row_max)
    weights = (raised / jnp.sum(raised, axis=-1, keepdims=True)).astype(jnp.bfloat16)
    result = jnp.einsum("hqk,khd->qhd", weights, values, preferred_element_type=jnp.float32)
    return result.astype(jnp.bfloat16)


def per_device(queries, latent, rope_key, latent_gain, kv_weight, gate, out_gain):
    own_tokens = queries.shape[0]
    groups = lax.axis_size("sp")
    seq_len = own_tokens * groups
    offset = lax.axis_index("sp") * own_tokens
    position = offset + jnp.arange(own_tokens, dtype=jnp.int32)
    widened = latent.astype(jnp.float32)
    normed = (
        widened * lax.rsqrt(jnp.mean(widened * widened, axis=-1, keepdims=True) + EPS) * latent_gain
    ).astype(jnp.bfloat16)
    keyval = jnp.dot(
        normed,
        lax.all_gather(kv_weight, "dp", axis=1, tiled=True),
        preferred_element_type=jnp.float32,
    ).astype(jnp.bfloat16)
    head_queries = queries.reshape(own_tokens, HEADS, NOPE + ROPE)
    head_queries = jnp.concatenate(
        [head_queries[..., :NOPE], rotary(head_queries[..., NOPE:], position)], axis=-1
    )
    head_queries = head_queries.reshape(own_tokens, HEADS * (NOPE + ROPE))
    rotated_all = gathered_copies(rotary(rope_key, position), "sp", 0)
    query_all, kv_all = (
        lax.all_to_all(head_queries, "sp", split_axis=1, concat_axis=0, tiled=True),
        lax.all_to_all(keyval, "sp", split_axis=1, concat_axis=0, tiled=True),
    )
    local_heads = HEADS // groups
    rows_all = query_all.shape[0]
    seq_count = rows_all // seq_len
    block_rows = min(512, seq_len)
    block_count = seq_len // block_rows

    def one_sequence(operands):
        query_seq, kv_seq, rope_seq = operands
        keys_plain = kv_seq[..., :NOPE]
        values = kv_seq[..., NOPE:]
        blocks = query_seq.reshape(block_count, block_rows, local_heads, NOPE + ROPE)
        result = lax.map(
            lambda piece_rows: attend(piece_rows, keys_plain, rope_seq, values), blocks
        )
        return result.reshape(seq_len, local_heads * VDIM)

    heads_out = lax.map(
        one_sequence,
        (
            query_all.reshape(seq_count, seq_len, local_heads, NOPE + ROPE),
            kv_all.reshape(seq_count, seq_len, local_heads, NOPE + VDIM),
            rotated_all.reshape(seq_count, seq_len, ROPE),
        ),
    )
    heads_out = heads_out.reshape(rows_all, local_heads * VDIM)
    token_rows = lax.all_to_all(heads_out, "sp", split_axis=0, concat_axis=1, tiled=True)
    gated_rows = token_rows.astype(jnp.float32) * jax.nn.silu(gate.astype(jnp.float32))
    scale_rows = lax.rsqrt(jnp.mean(gated_rows * gated_rows, axis=-1, keepdims=True) + EPS)
    return (gated_rows * scale_rows * out_gain).astype(jnp.bfloat16)


def solution(mesh):
    return jax.shard_map(
        per_device,
        mesh=mesh,
        in_specs=(
            P(("dp", "sp"), None),
            P(("dp", "sp"), None),
            P(("dp", "sp"), None),
            P(),
            P(None, "dp"),
            P(("dp", "sp"), None),
            P(),
        ),
        out_specs=P(("dp", "sp"), None),
        check_vma=False,
    )
```

profile of v0, /device:TPU:8, one launch (start us, length us, event | category | flops | bytes accessed | tf_op | source)
XLA Modules:
  0.0 278.0 jit_solution(5976931859334378445)
XLA Ops:
  8.4 11.7 %all-to-all-start.2 = ((bf16[32,128,64]{1,2,0:T(8,128)(2,1)}), bf16[32,128,64]{1,2,0:T(8,128)(2,1)S(1)}, u32[]{:S(2)}, u32[]{:S(2)}) async-start(bf16[32,128,64]{1,2,0:T(8,128)(2,1)} %broadcast_in_dim.7), calls=%async_computation.2 | async-start | bytes 1048576 | tf_op jit(solution)/shard_map/all_to_all | solution.py:22
  20.1 1.9 copy.26
  22.3 1.3 pad_maximum_fusion
  23.6 13.3 %all-to-all-done.2 = bf16[32,128,64]{1,2,0:T(8,128)(2,1)S(1)} async-done(((bf16[32,128,64]{1,2,0:T(8,128)(2,1)}), bf16[32,128,64]{1,2,0:T(8,128)(2,1)S(1)}, u32[]{:S(2)}, u32[]{:S(2)}) %all-to-all-start.2) | async-done | bytes 524320 | tf_op jit(solution)/shard_map/all_to_all | solution.py:22
  36.9 5.6 %all-to-all-start = ((bf16[128,32,192]{0,2,1:T(8,128)(2,1)}), bf16[128,32,192]{0,2,1:T(8,128)(2,1)S(1)}, u32[]{:S(2)}, u32[]{:S(2)}) async-start(bf16[128,32,192]{0,2,1:T(8,128)(2,1)} %pad_maximum_fusion), calls=%async_computation | async-start | bytes 3145728 | tf_op jit(solution)/shard_map/all_to_all | solution.py:85
  42.6 56.9 %all-gather.2.cloned.1.call-done = bf16[1024,8192]{1,0:T(8,128)(2,1)} async-done(((bf16[1024,1024]{1,0:T(8,128)(2,1)}), bf16[1024,8192]{1,0:T(8,128)(2,1)}) %all-gather.2.cloned.1.call-update) | async-done | bytes 16777232 | tf_op jit(solution)/shard_map/all_gather | solution.py:75
  99.5 8.2 %convolution_convert_fusion = bf16[128,8192]{1,0:T(8,128)(2,1)S(1)} fusion(bf16[1024,8192]{1,0:T(8,128)(2,1)} %all-gather.2.cloned.1.call-done, bf16[128,1024]{1,0:T(8,128)(2,1)S(1)} %copy-done.3, f32[1024]{0:T(1024)S(1)} %copy-done.8, f32[128]{0:T(128)S(1)} %add_rsqrt_fusion.1), kind=kOutput, calls=%fused_computation.16 | convolution fusion | flops 2149056512 | bytes 19141120 | tf_op jit(solution)/shard_map/dot_general | solution.py:73
  107.7 1.6 copy.39
  110.5 10.2 %all-to-all-start.1 = ((bf16[128,32,256]{2,0,1:T(8,128)(2,1)}), bf16[128,32,256]{2,0,1:T(8,128)(2,1)S(1)}, u32[]{:S(2)}, u32[]{:S(2)}) async-start(bf16[128,32,256]{2,0,1:T(8,128)(2,1)} %bitcast.86), calls=%async_computation.1 | async-start | bytes 4194304 | tf_op jit(solution)/shard_map/all_to_all | solution.py:86
  120.6 1.5 copy.35
  122.2 3.6 %copy.27 = bf16[32,128,192]{1,0,2:T(8,128)(2,1)} copy(bf16[32,128,192]{1,2,0:T(8,128)(2,1)} %bitcast.88) | data formatting | bytes 3145728 | tf_op jit(solution)/shard_map/all_to_all | solution.py:85
  125.7 3.7 %reshape.157 = bf16[8,512,1,192]{1,0,3,2:T(8,128)(2,1)} reshape(bf16[32,128,192]{1,0,2:T(8,128)(2,1)} %copy.27) | data formatting | bytes 3145728 | tf_op jit(solution)/shard_map/while/body/eval_jaxpr/reshape | solution.py:98
  129.5 3.1 %copy.30 = bf16[8,512,1,192]{1,3,2,0:T(8,128)(2,1)} copy(bf16[8,512,1,192]{1,0,3,2:T(8,128)(2,1)} %reshape.157) | data formatting | bytes 3145728 | tf_op jit(solution)/shard_map/while/body/eval_jaxpr/while | solution.py:99
  132.5 37.7 %all-to-all-done.1 = bf16[128,32,256]{2,0,1:T(8,128)(2,1)S(1)} async-done(((bf16[128,32,256]{2,0,1:T(8,128)(2,1)}), bf16[128,32,256]{2,0,1:T(8,128)(2,1)S(1)}, u32[]{:S(2)}, u32[]{:S(2)}) %all-to-all-start.1) | async-done | bytes 2097184 | tf_op jit(solution)/shard_map/all_to_all | solution.py:86
  170.2 1.3 copy-done
  171.6 2.7 fusion.35
  174.3 57.8 %while.17 = (s32[]{:T(128)}, bf16[8,512,1,128]{3,1,2,0:T(8,128)(2,1)S(1)}, bf16[8,512,1,192]{1,3,2,0:T(8,128)(2,1)}, bf16[4096,1,128]{2,0,1:T(8,128)(2,1)S(1)}, ...) while((s32[]{:T(128)}, bf16[8,512,1,128]{3,1,2,0:T(8,128)(2,1)S(1)}, ...), condition=%wide.region_4.5_spmd, body=%wide.region_1.4_spmd.sunk | while | flops 1359019008 | bytes 50014328 | solution.py:99
  175.3 1.3 fusion.50
  176.5 1.4 fusion.51
  178.0 1.3 fusion.52
  179.3 2.2 fusion.53
  182.5 1.3 fusion.50
  183.8 1.4 fusion.51
  185.2 1.3 fusion.52
  186.5 2.2 fusion.53
  189.7 1.3 fusion.50
  191.0 1.4 fusion.51
  192.4 1.3 fusion.52
  193.7 2.2 fusion.53
  196.9 1.3 fusion.50
  198.2 1.4 fusion.51
  199.7 1.3 fusion.52
  200.9 2.2 fusion.53
  204.2 1.3 fusion.50
  205.4 1.4 fusion.51
  208.2 2.2 fusion.53
  211.4 1.3 fusion.50
  212.7 1.4 fusion.51
  215.4 2.2 fusion.53
  218.6 1.3 fusion.50
  219.9 1.4 fusion.51
  222.6 2.2 fusion.53
  225.8 1.3 fusion.50
  227.1 1.4 fusion.51
  229.8 2.2 fusion.53
  233.1 6.3 %all-to-all-start.3 = ((bf16[32,128,128]{2,1,0:T(8,128)(2,1)}), bf16[32,128,128]{2,1,0:T(8,128)(2,1)S(1)}, u32[]{:S(2)}, u32[]{:S(2)}) async-start(bf16[32,128,128]{2,1,0:T(8,128)(2,1)} %bitcast.91), calls=%async_computation.3 | async-start | bytes 2097152 | tf_op jit(solution)/shard_map/all_to_all | solution.py:113
  240.1 27.4 %all-to-all-done.3 = bf16[32,128,128]{2,1,0:T(8,128)(2,1)S(1)} async-done(((bf16[32,128,128]{2,1,0:T(8,128)(2,1)}), bf16[32,128,128]{2,1,0:T(8,128)(2,1)S(1)}, u32[]{:S(2)}, u32[]{:S(2)}) %all-to-all-start.3) | async-done | bytes 1048608 | tf_op jit(solution)/shard_map/all_to_all | solution.py:113
  269.8 1.3 copy.34
  (65 shorter events, 19.9 us)
Async XLA Ops:
  6.5 0.8 copy-start.10
  6.5 93.0 %all-gather.2.cloned.1.call-start = ((), (), s32[]{:S(2)}) async-start(), calls=%async_computation.4 | async-start | bytes 18874368 | tf_op jit(solution)/shard_map/all_gather | solution.py:75
  8.4 28.5 %all-to-all-start.2 = ((bf16[32,128,64]{1,2,0:T(8,128)(2,1)}), bf16[32,128,64]{1,2,0:T(8,128)(2,1)S(1)}, u32[]{:S(2)}, u32[]{:S(2)}) async-start(bf16[32,128,64]{1,2,0:T(8,128)(2,1)} %broadcast_in_dim.7), calls=%async_computation.2 | async-start | bytes 1048576 | tf_op jit(solution)/shard_map/all_to_all | solution.py:22
  23.6 18.9 %copy-start.3 = (bf16[128,1024]{1,0:T(8,128)(2,1)S(1)}, bf16[128,1024]{1,0:T(8,128)(2,1)}, u32[]{:S(2)}) copy-start(bf16[128,1024]{1,0:T(8,128)(2,1)} %param.10) | copy-start | bytes 786436
  23.6 75.9 %copy-start.8 = (f32[1024]{0:T(1024)S(1)}, f32[1024]{0:T(1024)}, u32[]{:S(2)}) copy-start(f32[1024]{0:T(1024)} %param.12) | copy-start | bytes 12292
  36.9 70.8 %copy-start.2 = (bf16[32,128,64]{1,2,0:T(8,128)(2,1)}, bf16[32,128,64]{1,2,0:T(8,128)(2,1)S(1)}, u32[]{:S(2)}) copy-start(bf16[32,128,64]{1,2,0:T(8,128)(2,1)S(1)} %all-to-all-done.2) | copy-start | bytes 1572868
  36.9 72.4 %all-to-all-start = ((bf16[128,32,192]{0,2,1:T(8,128)(2,1)}), bf16[128,32,192]{0,2,1:T(8,128)(2,1)S(1)}, u32[]{:S(2)}, u32[]{:S(2)}) async-start(bf16[128,32,192]{0,2,1:T(8,128)(2,1)} %pad_maximum_fusion), calls=%async_computation | async-start | bytes 3145728 | tf_op jit(solution)/shard_map/all_to_all | solution.py:85
  109.3 1.2 copy-start.1
  110.5 59.8 %all-to-all-start.1 = ((bf16[128,32,256]{2,0,1:T(8,128)(2,1)}), bf16[128,32,256]{2,0,1:T(8,128)(2,1)S(1)}, u32[]{:S(2)}, u32[]{:S(2)}) async-start(bf16[128,32,256]{2,0,1:T(8,128)(2,1)} %bitcast.86), calls=%async_computation.1 | async-start | bytes 4194304 | tf_op jit(solution)/shard_map/all_to_all | solution.py:86
  170.2 1.3 copy-start
  171.6 2.7 copy-start.5
  178.0 1.3 copy-start.7
  185.2 1.3 copy-start.7
  192.4 1.3 copy-start.7
  199.7 1.3 copy-start.7
  206.9 1.3 copy-start.7
  214.1 1.3 copy-start.7
  221.3 1.3 copy-start.7
  228.6 1.3 copy-start.7
  232.1 1.0 copy-start.6
  232.1 7.3 %copy-start.4 = (bf16[128,4096]{1,0:T(8,128)(2,1)S(1)}, bf16[128,4096]{1,0:T(8,128)(2,1)}, u32[]{:S(2)}) copy-start(bf16[128,4096]{1,0:T(8,128)(2,1)} %param.14) | copy-start | bytes 3145732
  233.1 34.4 %all-to-all-start.3 = ((bf16[32,128,128]{2,1,0:T(8,128)(2,1)}), bf16[32,128,128]{2,1,0:T(8,128)(2,1)S(1)}, u32[]{:S(2)}, u32[]{:S(2)}) async-start(bf16[32,128,128]{2,1,0:T(8,128)(2,1)} %bitcast.91), calls=%async_computation.3 | async-start | bytes 2097152 | tf_op jit(solution)/shard_map/all_to_all | solution.py:113
  240.1 28.8 %copy-start.9 = (f32[4096]{0:T(1024)S(1)}, f32[4096]{0:T(1024)}, u32[]{:S(2)}) copy-start(f32[4096]{0:T(1024)} %param.15) | copy-start | bytes 49156
Sparse Core Ops, SparseCore 0:
  9.2 90.2 all-gather.1
where the time goes:
time: 279 us; the launch traced here: 278 us
  waiting for transfers between devices  136 us (49%)
  matrix products  47.9 us (17%)
  starting transfers between devices  33.8 us (12%)
  local copies, waits for them, and re-layouts  32.8 us (12%)
  other arithmetic  13.6 us (5%)
  between operations  13.6 us (5%)
    all_gather x1, waiting for transfers between devices, per_device(): lax.all_gather(kv_weight, 'dp', axis=1, tiled=True)  56.9 us
    all_to_all x1, waiting for transfers between devices, per_device(): lax.all_to_all(keyval, 'sp', split_axis=1, concat_axis=0, tiled=True)  37.7 us
    all_to_all x1, waiting for transfers between devices, per_device(): lax.all_to_all(heads_out, 'sp', split_axis=0, concat_axis=1, tiled=True)  27.4 us
    dot_general x8, matrix products, attend(): jnp.einsum('hqk,khd->qhd', weights, values, preferred_element_type=jnp.fl...  18 us
    all_to_all x1, waiting for transfers between devices, copy_for_each(): lax.all_to_all(jnp.broadcast_to(value[None], (length, *value.shape)), axi...  13.3 us
    all_to_all x1, starting transfers between devices, copy_for_each(): lax.all_to_all(jnp.broadcast_to(value[None], (length, *value.shape)), axi...  11.7 us
    dot_general x8, matrix products, attend(): jnp.einsum('qhr,kr->hqk', query_block[..., NOPE:], keys_rotated, preferre...  11.4 us
    dot_general x8, matrix products, attend(): jnp.einsum('qhd,khd->hqk', query_block[..., :NOPE], keys_plain, preferred...  10.3 us
  transfers between devices with their start and end apart: 5, of which 4 were waited for; matrix products, arithmetic and copies ran while one was open for 10% of the time, Pallas kernels for 0%

commit v1 on v0

--- a/solution.py
+++ b/solution.py
@@ -1,3 +1,4 @@
+import functools
 import jax
 import jax.numpy as jnp
 from jax import lax
@@ -9,6 +10,36 @@
 VDIM = 128
 EPS = 1e-06
 THETA = 10000.0
+
+
+def link_matrix_on_mesh(mine, device_axis):
+    out_arr = lax.axis_size(device_axis)
+    r_now = lax.axis_index(device_axis)
+    prior, f_now, state_next = (out_arr, r_now, mine.shape[1])
+    side_arr = range(prior)
+    z1 = map(lambda pp: (pp, (pp + 1) % prior), side_arr)
+    line_up = list(z1)
+    arr_out = range(prior)
+    u1 = map(lambda pp: (pp, (pp - 1) % prior), arr_out)
+    runs = list(u1)
+    frame_out = jnp.zeros((*mine.shape[:1], prior * state_next, *mine.shape[2:]), mine.dtype)
+    frame_out = lax.dynamic_update_slice_in_dim(frame_out, mine, f_now * state_next, axis=1)
+    new = built = mine
+    x_now = prior // 2
+    for j in tuple(range(1, x_now + 1)):
+        new = lax.ppermute(new, device_axis, perm=line_up)
+        frame_out = lax.dynamic_update_slice_in_dim(
+            frame_out, new, (f_now - j) % prior * state_next, axis=1
+        )
+        if j < prior - x_now:
+            built = lax.ppermute(built, axis_name=device_axis, perm=runs)
+            frame_out = lax.dynamic_update_slice_in_dim(
+                frame_out, built, (f_now + j) % prior * state_next, axis=1
+            )
+    return frame_out
+
+
+answer_the_pages = functools.partial(link_matrix_on_mesh, device_axis="dp")
 
 
 def in_order(blocks, dim):
@@ -71,9 +102,7 @@
         widened * lax.rsqrt(jnp.mean(widened * widened, axis=-1, keepdims=True) + EPS) * latent_gain
     ).astype(jnp.bfloat16)
     keyval = jnp.dot(
-        normed,
-        lax.all_gather(kv_weight, "dp", axis=1, tiled=True),
-        preferred_element_type=jnp.float32,
+        normed, answer_the_pages(kv_weight), preferred_element_type=jnp.float32
     ).astype(jnp.bfloat16)
     head_queries = queries.reshape(own_tokens, HEADS, NOPE + ROPE)
     head_queries = jnp.concatenate(

time: 279 us -> 292 us (1.047)
  the two profiles are of different devices: /device:TPU:8 before, /device:TPU:14 now
where the time goes in v1:
time: 292 us; the launch traced here: 291 us
  waiting for transfers between devices  146 us (50%)
  local copies, waits for them, and re-layouts  48.8 us (17%)
  matrix products  42.2 us (14%)
  starting transfers between devices  38.6 us (13%)
  other arithmetic  14.3 us (5%)
    ppermute x4, waiting for transfers between devices, link_matrix_on_mesh(): new = lax.ppermute(new, device_axis, perm=line_up)  56.9 us
    all_to_all x1, waiting for transfers between devices, per_device(): lax.all_to_all(keyval, 'sp', split_axis=1, concat_axis=0, tiled=True)  40.5 us
    all_to_all x1, waiting for transfers between devices, per_device(): lax.all_to_all(heads_out, 'sp', split_axis=0, concat_axis=1, tiled=True)  27.6 us
    all_to_all x1, waiting for transfers between devices, per_device(): lax.all_to_all(head_queries, 'sp', split_axis=1, concat_axis=0, tiled=True)  19.3 us
    dot_general x8, matrix products, attend(): jnp.einsum('hqk,khd->qhd', weights, values, preferred_element_type=jnp.fl...  18 us
    all_to_all x1, starting transfers between devices, copy_for_each(): lax.all_to_all(jnp.broadcast_to(value[None], (length, *value.shape)), axi...  11.7 us
    dot_general x8, matrix products, attend(): jnp.einsum('qhr,kr->hqk', query_block[..., NOPE:], keys_rotated, preferre...  11.4 us
    dot_general x8, matrix products, attend(): jnp.einsum('qhd,khd->hqk', query_block[..., :NOPE], keys_plain, preferred...  10.3 us
  transfers between devices with their start and end apart: 11, of which 7 were waited for; matrix products, arithmetic and copies ran while one was open for 12% of the time, Pallas kernels for 0%

profile of v1, /device:TPU:14, one launch (start us, length us, event | category | flops | bytes accessed | tf_op | source)
XLA Modules:
  0.0 290.9 jit_solution(5706441281551759901)
XLA Ops:
  0.0 1.7 collective-permute-start.1
  1.7 23.9 %collective-permute-done = bf16[1024,1024]{1,0:T(8,128)(2,1)S(1)} collective-permute-done((bf16[1024,1024]{1,0:T(8,128)(2,1)}, bf16[1024,1024]{1,0:T(8,128)(2,1)S(1)}, u32[]{:S(2)}, u32[]{:S(2)}) %collective-permute-start) | collective-permute-done | bytes 2097184 | tf_op jit(solution)/shard_map/ppermute | solution.py:30
  25.7 1.3 copy-done.4
  27.0 1.7 collective-permute-start.3
  28.8 23.8 %collective-permute-done.2 = bf16[1024,1024]{1,0:T(8,128)(2,1)} collective-permute-done((bf16[1024,1024]{1,0:T(8,128)(2,1)S(1)}, bf16[1024,1024]{1,0:T(8,128)(2,1)}, u32[]{:S(2)}, u32[]{:S(2)}) %collective-permute-start.2) | collective-permute-done | bytes 2097184 | tf_op jit(solution)/shard_map/ppermute | solution.py:30
  54.4 11.7 %all-to-all-start.2 = ((bf16[32,128,64]{1,2,0:T(8,128)(2,1)}), bf16[32,128,64]{1,2,0:T(8,128)(2,1)S(1)}, u32[]{:S(2)}, u32[]{:S(2)}) async-start(bf16[32,128,64]{1,2,0:T(8,128)(2,1)} %broadcast_in_dim.10), calls=%async_computation.2 | async-start | bytes 1048576 | tf_op jit(solution)/shard_map/all_to_all | solution.py:53
  66.1 1.9 copy.26
  69.2 9.1 %collective-permute-done.4 = bf16[1024,1024]{1,0:T(8,128)(2,1)} collective-permute-done((bf16[1024,1024]{1,0:T(8,128)(2,1)}, bf16[1024,1024]{1,0:T(8,128)(2,1)}, u32[]{:S(2)}, u32[]{:S(2)}) %collective-permute-start.4) | collective-permute-done | bytes 2097184 | tf_op jit(solution)/shard_map/ppermute | solution.py:30
  80.5 2.0 all-to-all-done.2
  82.4 9.9 %all-to-all-start = ((bf16[128,32,192]{0,2,1:T(8,128)(2,1)}), bf16[128,32,192]{0,2,1:T(8,128)(2,1)S(1)}, u32[]{:S(2)}, u32[]{:S(2)}) async-start(bf16[128,32,192]{0,2,1:T(8,128)(2,1)} %pad_maximum_fusion), calls=%async_computation | async-start | bytes 3145728 | tf_op jit(solution)/shard_map/all_to_all | solution.py:114
  92.6 1.6 broadcast_in_dim.9
  96.1 1.9 constant_dynamic-update-slice_fusion.5
  98.0 1.9 constant_dynamic-update-slice_fusion.4
  99.9 1.9 constant_dynamic-update-slice_fusion.3
  101.7 1.9 constant_dynamic-update-slice_fusion.2
  103.6 1.9 constant_dynamic-update-slice_fusion.1
  105.5 1.9 constant_dynamic-update-slice_fusion
  107.4 2.5 convolution_convert_fusion
  109.9 1.6 copy.39
  111.5 19.3 %all-to-all-done = bf16[128,32,192]{0,2,1:T(8,128)(2,1)S(1)} async-done(((bf16[128,32,192]{0,2,1:T(8,128)(2,1)}), bf16[128,32,192]{0,2,1:T(8,128)(2,1)S(1)}, u32[]{:S(2)}, u32[]{:S(2)}) %all-to-all-start) | async-done | bytes 1572896 | tf_op jit(solution)/shard_map/all_to_all | solution.py:114
  131.9 6.2 %all-to-all-start.1 = ((bf16[128,32,256]{2,0,1:T(8,128)(2,1)}), bf16[128,32,256]{2,0,1:T(8,128)(2,1)S(1)}, u32[]{:S(2)}, u32[]{:S(2)}) async-start(bf16[128,32,256]{2,0,1:T(8,128)(2,1)} %bitcast.86), calls=%async_computation.1 | async-start | bytes 4194304 | tf_op jit(solution)/shard_map/all_to_all | solution.py:115
  138.2 1.5 copy.35
  139.7 3.6 %copy.27 = bf16[32,128,192]{1,0,2:T(8,128)(2,1)} copy(bf16[32,128,192]{1,2,0:T(8,128)(2,1)} %bitcast.88) | data formatting | bytes 3145728 | tf_op jit(solution)/shard_map/all_to_all | solution.py:114
  143.3 3.7 %reshape.157 = bf16[8,512,1,192]{1,0,3,2:T(8,128)(2,1)} reshape(bf16[32,128,192]{1,0,2:T(8,128)(2,1)} %copy.27) | data formatting | bytes 3145728 | tf_op jit(solution)/shard_map/while/body/eval_jaxpr/reshape | solution.py:127
  147.0 3.0 %copy.30 = bf16[8,512,1,192]{1,3,2,0:T(8,128)(2,1)} copy(bf16[8,512,1,192]{1,0,3,2:T(8,128)(2,1)} %reshape.157) | data formatting | bytes 3145728 | tf_op jit(solution)/shard_map/while/body/eval_jaxpr/while | solution.py:128
  150.0 40.5 %all-to-all-done.1 = bf16[128,32,256]{2,0,1:T(8,128)(2,1)S(1)} async-done(((bf16[128,32,256]{2,0,1:T(8,128)(2,1)}), bf16[128,32,256]{2,0,1:T(8,128)(2,1)S(1)}, u32[]{:S(2)}, u32[]{:S(2)}) %all-to-all-start.1) | async-done | bytes 2097184 | tf_op jit(solution)/shard_map/all_to_all | solution.py:115
  190.6 1.3 copy-done
  191.9 2.8 fusion.35
  194.7 57.8 %while.17 = (s32[]{:T(128)}, bf16[8,512,1,128]{3,1,2,0:T(8,128)(2,1)S(1)}, bf16[8,512,1,192]{1,3,2,0:T(8,128)(2,1)}, bf16[4096,1,128]{2,0,1:T(8,128)(2,1)S(1)}, ...) while((s32[]{:T(128)}, bf16[8,512,1,128]{3,1,2,0:T(8,128)(2,1)S(1)}, ...), condition=%wide.region_4.5_spmd, body=%wide.region_1.4_spmd.sunk | while | flops 1359019008 | bytes 50014320 | solution.py:128
  196.9 1.4 fusion.51
  199.6 2.2 fusion.53
  204.1 1.4 fusion.51
  206.8 2.2 fusion.53
  211.3 1.4 fusion.51
  214.1 2.2 fusion.53
  218.6 1.4 fusion.51
  221.3 2.2 fusion.53
  225.8 1.4 fusion.51
  228.5 2.2 fusion.53
  233.0 1.4 fusion.51
  235.7 2.2 fusion.53
  240.2 1.4 fusion.51
  243.0 2.2 fusion.53
  247.5 1.4 fusion.51
  250.2 2.2 fusion.53
  253.4 5.6 %all-to-all-start.3 = ((bf16[32,128,128]{2,1,0:T(8,128)(2,1)}), bf16[32,128,128]{2,1,0:T(8,128)(2,1)S(1)}, u32[]{:S(2)}, u32[]{:S(2)}) async-start(bf16[32,128,128]{2,1,0:T(8,128)(2,1)} %bitcast.91), calls=%async_computation.3 | async-start | bytes 2097152 | tf_op jit(solution)/shard_map/all_to_all | solution.py:142
  259.7 27.6 %all-to-all-done.3 = bf16[32,128,128]{2,1,0:T(8,128)(2,1)S(1)} async-done(((bf16[32,128,128]{2,1,0:T(8,128)(2,1)}), bf16[32,128,128]{2,1,0:T(8,128)(2,1)S(1)}, u32[]{:S(2)}, u32[]{:S(2)}) %all-to-all-start.3) | async-done | bytes 1048608 | tf_op jit(solution)/shard_map/all_to_all | solution.py:142
  289.6 1.3 copy.34
  (89 shorter events, 40.2 us)
Async XLA Ops:
  0.0 25.7 %collective-permute-start = (bf16[1024,1024]{1,0:T(8,128)(2,1)}, bf16[1024,1024]{1,0:T(8,128)(2,1)S(1)}, u32[]{:S(2)}, u32[]{:S(2)}) collective-permute-start(bf16[1024,1024]{1,0:T(8,128)(2,1)} %param.13), channel_id=1, source_target_pairs={{0,1},{1,2},{2,3},{3,4},{4,5},{5,6},{6,7},{7,0},{8,9},{9,10},{10,1... | collective-permute-start | bytes 6291464 | tf_op jit(solution)/shard_map/ppermute | solution.py:30
  0.0 27.0 %collective-permute-start.1 = (bf16[1024,1024]{1,0:T(8,128)(2,1)}, bf16[1024,1024]{1,0:T(8,128)(2,1)}, u32[]{:S(2)}, u32[]{:S(2)}) collective-permute-start(bf16[1024,1024]{1,0:T(8,128)(2,1)} %param.13), channel_id=1, source_target_pairs={{0,7},{1,0},{2,1},{3,2},{4,3},{5,4},{6,5},{7,6},{8,15},{9,8},{10,9... | collective-permute-start | bytes 6291464 | tf_op jit(solution)/shard_map/ppermute | solution.py:35
  25.7 1.3 copy-start.4
  27.0 25.6 %collective-permute-start.2 = (bf16[1024,1024]{1,0:T(8,128)(2,1)S(1)}, bf16[1024,1024]{1,0:T(8,128)(2,1)}, u32[]{:S(2)}, u32[]{:S(2)}) collective-permute-start(bf16[1024,1024]{1,0:T(8,128)(2,1)S(1)} %collective-permute-done), channel_id=1, source_target_pairs={{0,1},{1,2},{2,3},{3,4},{4,5},{5,6},{6,7},{7,0},{8,9},{9,10},{10,1... | collective-permute-start | bytes 6291464 | tf_op jit(solution)/shard_map/ppermute | solution.py:30
  27.0 41.0 %collective-permute-start.3 = (bf16[1024,1024]{1,0:T(8,128)(2,1)}, bf16[1024,1024]{1,0:T(8,128)(2,1)}, u32[]{:S(2)}, u32[]{:S(2)}) collective-permute-start(bf16[1024,1024]{1,0:T(8,128)(2,1)} %collective-permute-done.1), channel_id=1, source_target_pairs={{0,7},{1,0},{2,1},{3,2},{4,3},{5,4},{6,5},{7,6},{8,15},{9,8},{10,9... | collective-permute-start | bytes 6291464 | tf_op jit(solution)/shard_map/ppermute | solution.py:35
  52.6 25.8 %collective-permute-start.4 = (bf16[1024,1024]{1,0:T(8,128)(2,1)}, bf16[1024,1024]{1,0:T(8,128)(2,1)}, u32[]{:S(2)}, u32[]{:S(2)}) collective-permute-start(bf16[1024,1024]{1,0:T(8,128)(2,1)} %collective-permute-done.2), channel_id=1, source_target_pairs={{0,1},{1,2},{2,3},{3,4},{4,5},{5,6},{6,7},{7,0},{8,9},{9,10},{10,1... | collective-permute-start | bytes 6291464 | tf_op jit(solution)/shard_map/ppermute | solution.py:30
  54.4 28.0 %all-to-all-start.2 = ((bf16[32,128,64]{1,2,0:T(8,128)(2,1)}), bf16[32,128,64]{1,2,0:T(8,128)(2,1)S(1)}, u32[]{:S(2)}, u32[]{:S(2)}) async-start(bf16[32,128,64]{1,2,0:T(8,128)(2,1)} %broadcast_in_dim.10), calls=%async_computation.2 | async-start | bytes 1048576 | tf_op jit(solution)/shard_map/all_to_all | solution.py:53
  68.0 35.6 %collective-permute-start.5 = (bf16[1024,1024]{1,0:T(8,128)(2,1)}, bf16[1024,1024]{1,0:T(8,128)(2,1)}, u32[]{:S(2)}, u32[]{:S(2)}) collective-permute-start(bf16[1024,1024]{1,0:T(8,128)(2,1)} %collective-permute-done.3), channel_id=1, source_target_pairs={{0,7},{1,0},{2,1},{3,2},{4,3},{5,4},{6,5},{7,6},{8,15},{9,8},{10,9... | collective-permute-start | bytes 6291464 | tf_op jit(solution)/shard_map/ppermute | solution.py:35
  78.3 27.2 %collective-permute-start.6 = (bf16[1024,1024]{1,0:T(8,128)(2,1)}, bf16[1024,1024]{1,0:T(8,128)(2,1)}, u32[]{:S(2)}, u32[]{:S(2)}) collective-permute-start(bf16[1024,1024]{1,0:T(8,128)(2,1)} %collective-permute-done.4), channel_id=1, source_target_pairs={{0,1},{1,2},{2,3},{3,4},{4,5},{5,6},{6,7},{7,0},{8,9},{9,10},{10,1... | collective-permute-start | bytes 6291464 | tf_op jit(solution)/shard_map/ppermute | solution.py:30
  80.5 12.0 %copy-start.6 = (bf16[128,1024]{1,0:T(8,128)(2,1)S(1)}, bf16[128,1024]{1,0:T(8,128)(2,1)}, u32[]{:S(2)}) copy-start(bf16[128,1024]{1,0:T(8,128)(2,1)} %param.10) | copy-start | bytes 786436
  82.4 11.8 %copy-start.2 = (bf16[32,128,64]{1,2,0:T(8,128)(2,1)}, bf16[32,128,64]{1,2,0:T(8,128)(2,1)S(1)}, u32[]{:S(2)}) copy-start(bf16[32,128,64]{1,2,0:T(8,128)(2,1)S(1)} %all-to-all-done.2) | copy-start | bytes 1572868
  82.4 48.4 %all-to-all-start = ((bf16[128,32,192]{0,2,1:T(8,128)(2,1)}), bf16[128,32,192]{0,2,1:T(8,128)(2,1)S(1)}, u32[]{:S(2)}, u32[]{:S(2)}) async-start(bf16[128,32,192]{0,2,1:T(8,128)(2,1)} %pad_maximum_fusion), calls=%async_computation | async-start | bytes 3145728 | tf_op jit(solution)/shard_map/all_to_all | solution.py:114
  92.6 1.7 copy-start.3
  94.3 1.6 copy-start.5
  105.5 1.9 copy-start.11
  130.8 1.1 copy-start.1
  131.9 58.7 %all-to-all-start.1 = ((bf16[128,32,256]{2,0,1:T(8,128)(2,1)}), bf16[128,32,256]{2,0,1:T(8,128)(2,1)S(1)}, u32[]{:S(2)}, u32[]{:S(2)}) async-start(bf16[128,32,256]{2,0,1:T(8,128)(2,1)} %bitcast.86), calls=%async_computation.1 | async-start | bytes 4194304 | tf_op jit(solution)/shard_map/all_to_all | solution.py:115
  190.6 1.3 copy-start
  191.9 2.8 copy-start.8
  198.3 1.3 copy-start.10
  205.5 1.3 copy-start.10
  212.8 1.3 copy-start.10
  220.0 1.3 copy-start.10
  227.2 1.3 copy-start.10
  234.4 1.3 copy-start.10
  241.7 1.3 copy-start.10
  248.9 1.3 copy-start.10
  252.5 1.0 copy-start.9
  252.5 6.6 %copy-start.7 = (bf16[128,4096]{1,0:T(8,128)(2,1)S(1)}, bf16[128,4096]{1,0:T(8,128)(2,1)}, u32[]{:S(2)}) copy-start(bf16[128,4096]{1,0:T(8,128)(2,1)} %param.14) | copy-start | bytes 3145732
  253.4 33.9 %all-to-all-start.3 = ((bf16[32,128,128]{2,1,0:T(8,128)(2,1)}), bf16[32,128,128]{2,1,0:T(8,128)(2,1)S(1)}, u32[]{:S(2)}, u32[]{:S(2)}) async-start(bf16[32,128,128]{2,1,0:T(8,128)(2,1)} %bitcast.91), calls=%async_computation.3 | async-start | bytes 2097152 | tf_op jit(solution)/shard_map/all_to_all | solution.py:142
  259.7 29.0 %copy-start.12 = (f32[4096]{0:T(1024)S(1)}, f32[4096]{0:T(1024)}, u32[]{:S(2)}) copy-start(f32[4096]{0:T(1024)} %param.15) | copy-start | bytes 49156
